TPU v7x, 32 devices: a whole 2x2x4 slice. The times are simulated.
32 devices in a mesh: sp: 16 (over z, y, x), tp: 2 (over core).
Axes of the slice: x: 2, y: 2, z: 4, core: 2. Of those that a mesh axis runs over, the one named last changes fastest.
Arguments:
- residual: bfloat16 [2048, 2048], P(('sp', 'tp')), may hold values from -6 to 6
- conv_input: bfloat16 [2048, 1024], P('sp', 'tp'), may hold values from -6 to 6
- input_gate: bfloat16 [2048, 1024], P('sp', 'tp'), may hold values from -6 to 6
- output_gate: bfloat16 [2048, 1024], P('sp', 'tp'), may hold values from -6 to 6
- conv_taps: bfloat16 [3, 1024], P(None, 'tp'), may hold values from -3.5 to 3.5
- out_proj: bfloat16 [1024, 2048], P('tp'), may hold values from -0.1875 to 0.1875
- norm_gain: float32 [2048], replicated, may hold values from 0.1 to 1.9
- routes: int32 [2048, 2], P(('sp', 'tp')), may hold values from 0 to 15, all different within a row; in each aligned block of 64 rows (0 to 63, 64 to 127, ...) at most 16 rows name the same one
- route_weight: float32 [2048, 2], P(('sp', 'tp')), may hold values from 0.1 to 1
- gate_proj: bfloat16 [16, 2048, 3584], P('sp', None, 'tp'), may hold values from -0.125 to 0.125
- up_proj: bfloat16 [16, 2048, 3584], P('sp', None, 'tp'), may hold values from -0.125 to 0.125
- down_proj: bfloat16 [16, 3584, 2048], P('sp', 'tp'), may hold values from -0.09375 to 0.09375
Outputs:
- layer_out: bfloat16 [2048, 2048], P(('sp', 'tp'))
Inputs may be any that keep to these rules, and one draw needn't show every extreme that they name: `routes`: A token's 2 experts differ. Among the 64 tokens of one device, in the aligned blocks of the tokens' order, no expert is named more than 16 times, a bound that some block reaches in some device.
All inputs are finite; a program needn't handle non-finite values.
Results may differ from a plain program's by a relative error of at most 0.0054.
Values may be sent and summed in bfloat16 or wider, within the bound.
A program may use at most 128 MiB of HBM per device.

v0:
```python
import functools

import jax
import jax.numpy as jnp
from jax import lax
from jax.experimental import pallas as pl
from jax.experimental.pallas import tpu as pltpu
from jax.sharding import PartitionSpec as P

MESH = pl.DeviceIdType.MESH
F32 = jnp.float32
BF16 = jnp.bfloat16
RIM = 16


IN_TILE = 1792
OUT_TILE = 1024


def tile_of(size, most):
    for tile in range(most, 127, -128):
        if size % tile == 0:
            return tile
    return size


def dot(a, b):
    return jnp.dot(a, b, preferred_element_type=F32)


def kernel(
    peers,
    groups,
    rows,
    residual,
    conv_input,
    input_gate,
    output_gate,
    taps,
    gain,
    routes,
    weights,
    out_proj_hbm,
    gate_hbm,
    up_hbm,
    down_hbm,
    out,
    out_proj,
    gate,
    up,
    down,
    rim,
    ext,
    chosen,
    proj,
    proj_in,
    outgoing,
    recv,
    active,
    part,
    part_in,
    ret,
    spread,
    load_sem,
    rim_send,
    rim_recv,
    proj_send,
    proj_recv,
    out_send,
    out_recv,
    fwd_send,
    fwd_recv,
    part_send,
    part_recv,
    ret_send,
    ret_recv,
):
    me = lax.axis_index("sp")
    core = lax.axis_index("tp")
    other = 1 - core
    length, channels = conv_input.shape
    tokens, width = residual.shape
    hidden = gate.shape[1]
    tap_count = taps.shape[0]
    per_group = peers // groups

    loads = []
    for i, (src, dst) in enumerate(
        ((out_proj_hbm, out_proj), (gate_hbm.at[0], gate), (up_hbm.at[0], up), (down_hbm.at[0], down))
    ):
        load = pltpu.make_async_copy(src, dst, load_sem.at[i])
        load.start()
        loads.append(load)

    barrier = pltpu.get_barrier_semaphore()

    @pl.loop(1, peers)
    def _(k):
        pl.semaphore_signal(
            barrier, inc=1, device_id=(lax.rem(me + k, peers), core), device_id_type=MESH
        )

    pl.semaphore_signal(barrier, inc=1, device_id=(me, other), device_id_type=MESH)
    tops = routes.shape[0]
    ids = lax.broadcasted_iota(jnp.int32, (peers, tokens), 0)
    hots = [(routes[k : k + 1, :] == ids).astype(F32) for k in range(tops)]
    total = functools.reduce(jnp.add, hots)
    earlier = (
        lax.broadcasted_iota(jnp.int32, (tokens, tokens), 0)
        < lax.broadcasted_iota(jnp.int32, (tokens, tokens), 1)
    ).astype(BF16)
    counts = dot(total.astype(BF16), earlier)
    lines = lax.broadcasted_iota(jnp.int32, (peers * rows, tokens), 0)
    select = jnp.zeros((peers * rows, tokens), F32)
    weigh = jnp.zeros((peers * rows, tokens), F32)
    for k in range(tops):
        slot = jnp.sum(counts * hots[k], axis=0, keepdims=True).astype(jnp.int32)
        hit = lines == routes[k : k + 1, :] * rows + slot
        select = jnp.where(hit, 1.0, select)
        weigh = jnp.where(hit, weights[k : k + 1, :], weigh)
    chosen[...] = select.astype(BF16)
    half = per_group * rows
    for g in range(groups):
        rest = weigh[g * half : (g + 1) * half].T
        pieces = []
        for _ in range(3):
            piece = rest.astype(BF16).astype(F32)
            pieces.append(piece)
            rest = rest - piece
        spread[g] = jnp.concatenate(pieces, axis=1).astype(BF16)

    ext[pl.ds(RIM, length)] = input_gate[...].astype(F32) * conv_input[...].astype(F32)

    def gate_rows(lane):
        convolved = jnp.zeros((tokens, channels), F32)
        for j in range(tap_count):
            convolved = convolved + taps[j : j + 1, :].astype(F32) * ext[
                pl.ds(RIM - tap_count + 1 + j + lane * tokens, tokens)
            ]
        opened = output_gate[pl.ds(lane * tokens, tokens)].astype(F32)
        return (opened * convolved).astype(BF16)

    late = gate_rows(1)
    loads[0].wait()
    proj[1] = dot(late, out_proj[...])

    pl.semaphore_wait(barrier, peers)

    def rim_copy(which, target):
        src = (conv_input, input_gate)[which]
        return pltpu.make_async_remote_copy(
            src_ref=src.at[pl.ds(length - RIM, RIM)],
            dst_ref=rim.at[which],
            send_sem=rim_send.at[which],
            recv_sem=rim_recv.at[which],
            device_id=(target, core),
            device_id_type=MESH,
        )

    @pl.when(me < peers - 1)
    def _():
        for which in range(2):
            rim_copy(which, me + 1).start()

    proj_copy = pltpu.make_async_remote_copy(
        src_ref=proj.at[other],
        dst_ref=proj_in,
        send_sem=proj_send,
        recv_sem=proj_recv,
        device_id=(me, other),
        device_id_type=MESH,
    )

    @pl.when(core == 0)
    def _():
        proj_copy.start()

    @pl.when(me == 0)
    def _():
        ext[pl.ds(0, RIM)] = jnp.zeros((RIM, channels), F32)

    @pl.when(me > 0)
    def _():
        for which in range(2):
            rim_copy(which, me).wait_recv()
        ext[pl.ds(0, RIM)] = rim[1].astype(F32) * rim[0].astype(F32)

    proj[0] = dot(gate_rows(0), out_proj[...])

    @pl.when(core == 1)
    def _():
        proj_copy.start()

    proj_copy.wait_recv()
    stream = residual[...].astype(F32) + (proj[core] + proj_in[...])
    inverse_rms = lax.rsqrt(jnp.mean(stream * stream, axis=-1, keepdims=True) + 1e-06)
    normed = (stream * inverse_rms * gain[...]).astype(BF16)
    proj_copy.wait_send()
    proj[core] = stream
    outgoing[...] = dot(chosen[...], normed).astype(BF16).reshape(peers, rows, width)

    def out_copy(slot, src, target):
        return pltpu.make_async_remote_copy(
            src_ref=outgoing.at[slot],
            dst_ref=recv.at[core, src],
            send_sem=out_send.at[slot],
            recv_sem=out_recv.at[src],
            device_id=(target, core),
            device_id_type=MESH,
        )

    mine = me // per_group
    if groups == 4:
        near = mine // 2 * 2
        far = lax.rem(near + 2, 4)
        side = mine - near
        order = [(far + side, 1), (far + 1 - side, 1)]
        if active.shape[0] > 2 * half:
            order = [(near, 2)] + order
        else:
            order = [(mine, 1), (near + 1 - side, 1)] + order
    else:
        order = [(lax.rem(mine + step, groups), 1) for step in range(groups)]
    order = [(group * per_group, count * per_group) for group, count in order]

    for first, count in order:

        @pl.loop(0, count)
        def _(i):
            target = first + lax.rem(me + i, count)

            @pl.when(target != me)
            def _():
                out_copy(target, me, target).start()

    recv[core, me] = outgoing[me]
    loads[1].wait()
    loads[2].wait()
    loads[3].wait()

    def fwd_copy(src, lane):
        return pltpu.make_async_remote_copy(
            src_ref=recv.at[lane, src],
            dst_ref=recv.at[lane, src],
            send_sem=fwd_send.at[src],
            recv_sem=fwd_recv.at[src],
            device_id=(me, other),
            device_id_type=MESH,
        )

    def ret_copy(src, slot, target):
        return pltpu.make_async_remote_copy(
            src_ref=part.at[core, src],
            dst_ref=ret.at[slot],
            send_sem=ret_send.at[src],
            recv_sem=ret_recv.at[slot],
            device_id=(target, core),
            device_id_type=MESH,
        )

    in_tile = tile_of(hidden, IN_TILE)
    out_tile = tile_of(width // 2, OUT_TILE)

    for step, (first, count) in enumerate(order):
        span = pl.ds(first, count)
        lot = count * rows

        @pl.loop(0, count)
        def _(i):
            src = first + lax.rem(me + i, count)

            @pl.when(src != me)
            def _():
                out_copy(src, src, src).wait_recv()

            fwd_copy(src, core).start()

        @pl.loop(0, count)
        def _(i):
            fwd_copy(first + lax.rem(me + i, count), other).wait_recv()

        @pl.loop(0, hidden // in_tile)
        def _(n):
            cols = pl.ds(pl.multiple_of(n * in_tile, in_tile), in_tile)
            x = recv[:, span].reshape(2 * lot, width)
            g = dot(x, gate[:, cols])
            u = dot(x, up[:, cols])
            active[pl.ds(0, 2 * lot), cols] = (g * (1.0 / (1.0 + jnp.exp(-g))) * u).astype(BF16)

        copies = []
        for side_of in range(2):
            start = side_of * (width // 2)

            @pl.loop(0, width // 2 // out_tile)
            def _(n):
                cols = pl.ds(pl.multiple_of(start + n * out_tile, 128), out_tile)
                y = dot(active[pl.ds(0, 2 * lot)], down[:, cols]).astype(BF16)
                part[:, span, :, cols] = y.reshape(2, count, rows, out_tile)

            part_half = pl.ds(start, width // 2)
            copy = pltpu.make_async_remote_copy(
                src_ref=part.at[other, span, :, part_half],
                dst_ref=part_in.at[span, :, part_half],
                send_sem=part_send.at[step, side_of],
                recv_sem=part_recv.at[step, side_of],
                device_id=(me, other),
                device_id_type=MESH,
            )
            copy.start()
            copies.append(copy)
        for copy in copies:
            copy.wait()

        @pl.loop(0, count)
        def _(i):
            src = first + lax.rem(me + i, count)
            halves = (part[core, src].astype(F32) + part_in[src].astype(F32)).astype(BF16)
            part[core, src] = halves

            @pl.when(src != me)
            def _():
                ret_copy(src, me, src).start()

            @pl.when(src == me)
            def _():
                ret[me] = halves

    for step, (first, count) in enumerate(order):

        @pl.loop(0, count)
        def _(i):
            src = first + i

            @pl.when(src != me)
            def _():
                ret_copy(src, src, src).wait_recv()

        for n in range(width // out_tile):
            cols = pl.ds(n * out_tile, out_tile)
            added = proj[core, :, cols]
            for g in range(count // per_group):
                values = ret[pl.ds(first + g * per_group, per_group), :, cols]
                values = values.reshape(half, out_tile)
                added = added + dot(
                    spread[first // per_group + g], jnp.concatenate([values] * 3, axis=0)
                )
            if step < len(order) - 1:
                proj[core, :, cols] = added
            else:
                out[:, cols] = added.astype(BF16)

    @pl.loop(0, peers)
    def _(src):
        @pl.when(src != me)
        def _():
            out_copy(src, src, src).wait_send()
            ret_copy(src, src, src).wait_send()

        fwd_copy(src, core).wait_send()

    @pl.when(me < peers - 1)
    def _():
        for which in range(2):
            rim_copy(which, me + 1).wait_send()


def per_device(
    residual,
    conv_input,
    input_gate,
    output_gate,
    conv_taps,
    out_proj,
    norm_gain,
    routes,
    route_weight,
    gate_proj,
    up_proj,
    down_proj,
):
    peers = lax.axis_size("sp")
    tokens, width = residual.shape
    length, channels = conv_input.shape
    hidden = gate_proj.shape[2]
    capacity = 2 * tokens * routes.shape[1] // peers
    rows = -(-capacity // 16) * 16
    groups = 4 if peers % 4 == 0 else 1
    half = peers // groups * rows
    joined = 2 if groups == 4 and half <= 64 else 1
    dma = pltpu.SemaphoreType.DMA
    vmem = pl.BlockSpec(memory_space=pltpu.VMEM)
    hbm = pl.BlockSpec(memory_space=pltpu.HBM)
    return pl.pallas_call(
        functools.partial(kernel, peers, groups, rows),
        out_shape=jax.ShapeDtypeStruct((tokens, width), BF16),
        in_specs=[vmem] * 8 + [hbm] * 4,
        out_specs=vmem,
        scratch_shapes=[
            pltpu.VMEM(out_proj.shape, BF16),
            pltpu.VMEM(gate_proj.shape[1:], BF16),
            pltpu.VMEM(up_proj.shape[1:], BF16),
            pltpu.VMEM(down_proj.shape[1:], BF16),
            pltpu.VMEM((2, RIM, channels), BF16),
            pltpu.VMEM((RIM + length, channels), F32),
            pltpu.VMEM((peers * rows, tokens), BF16),
            pltpu.VMEM((2, tokens, width), F32),
            pltpu.VMEM((tokens, width), F32),
            pltpu.VMEM((peers, rows, width), BF16),
            pltpu.VMEM((2, peers, rows, width), BF16),
            pltpu.VMEM((2 * joined * half, hidden), BF16),
            pltpu.VMEM((2, peers, rows, width), BF16),
            pltpu.VMEM((peers, rows, width), BF16),
            pltpu.VMEM((peers, rows, width), BF16),
            pltpu.VMEM((groups, tokens, 3 * half), BF16),
            dma((4,)),
            dma((2,)),
            dma((2,)),
            dma,
            dma,
            dma((peers,)),
            dma((peers,)),
            dma((peers,)),
            dma((peers,)),
            dma((groups, 2)),
            dma((groups, 2)),
            dma((peers,)),
            dma((peers,)),
        ],
        compiler_params=pltpu.CompilerParams(
            collective_id=0, has_side_effects=True, vmem_limit_bytes=67043328
        ),
        name="mixer_experts",
    )(
        residual,
        conv_input,
        input_gate,
        output_gate,
        conv_taps,
        norm_gain.reshape(1, width),
        routes.T,
        route_weight.T,
        out_proj,
        gate_proj,
        up_proj,
        down_proj,
    )


def solution(mesh):
    return jax.shard_map(
        per_device,
        mesh=mesh,
        in_specs=(
            P(("sp", "tp"), None),
            P("sp", "tp"),
            P("sp", "tp"),
            P("sp", "tp"),
            P(None, "tp"),
            P("tp", None),
            P(),
            P(("sp", "tp"), None),
            P(("sp", "tp"), None),
            P("sp", None, "tp"),
            P("sp", None, "tp"),
            P("sp", "tp", None),
        ),
        out_specs=P(("sp", "tp"), None),
        check_vma=False,
    )
```

profile of v0, /device:TPU:12, one launch (start us, length us, event | category | flops | bytes accessed | tf_op | source)
XLA Modules:
  0.0 62.1 jit_solution(16894368740770091384)
XLA Ops:
  0.0 60.5 %mixer_experts.1 = bf16[64,2048]{1,0:T(8,128)(2,1)} custom-call(bf16[64,2048]{1,0:T(8,128)(2,1)} %residual.1, bf16[128,512]{1,0:T(8,128)(2,1)} %conv_input.1, bf16[128,512]{1,0:T(8,128)(2,1)} %input_gate.1, bf16[128,512]{1,0:T(8,128)(2,1)} %output_gate.1, bf16[3,512]{1,0:T(4,128)(2,1)} %taps.1, f32[1,2048]{1,0:T(1,128)} %bitcast.3, s32[2,64]{1,0:T(2,128)} %bitcast.4, ...), custom_call_target="tpu_custom_call" | custom-call | tf_op jit(solution)/shard_map/mixer_experts/pallas_call | solution.py:393
  60.5 1.7 %copy.14 = bf16[64,2048]{1,0:T(8,128)(2,1)} copy(bf16[64,2048]{1,0:T(8,128)(2,1)} %mixer_experts.1) | data formatting | bytes 524288
where the time goes:
time: 62.3 us; the launch traced here: 62.1 us
  Pallas kernels  60.5 us (97%)
  local copies, waits for them, and re-layouts  1.67 us (3%)
    pallas_call x1, Pallas kernels, per_device(): pl.pallas_call(functools.partial(kernel, peers, groups, rows), out_shape=...  60.5 us
    unnamed x1, local copies, waits for them, and re-layouts  1.67 us

commit v1 on v0

--- a/solution.py
+++ b/solution.py
@@ -32,6 +32,19 @@
     peers,
     groups,
     rows,
+    residual_hbm,
+    conv_input_hbm,
+    input_gate_hbm,
+    output_gate_hbm,
+    taps_hbm,
+    gain_hbm,
+    routes_hbm,
+    weights_hbm,
+    out_proj_hbm,
+    gate_hbm,
+    up_hbm,
+    down_hbm,
+    out,
     residual,
     conv_input,
     input_gate,
@@ -40,11 +53,6 @@
     gain,
     routes,
     weights,
-    out_proj_hbm,
-    gate_hbm,
-    up_hbm,
-    down_hbm,
-    out,
     out_proj,
     gate,
     up,
@@ -54,6 +62,9 @@
     chosen,
     proj,
     proj_in,
+    raw,
+    raw_in,
+    chosen_in,
     outgoing,
     recv,
     active,
@@ -66,6 +77,10 @@
     rim_recv,
     proj_send,
     proj_recv,
+    raw_send,
+    raw_recv,
+    chosen_send,
+    chosen_recv,
     out_send,
     out_recv,
     fwd_send,
@@ -84,23 +99,39 @@
     tap_count = taps.shape[0]
     per_group = peers // groups
 
+    barrier = pltpu.get_barrier_semaphore()
+
+    @pl.loop(1, peers)
+    def _(k):
+        pl.semaphore_signal(
+            barrier, inc=1, device_id=(lax.rem(me + k, peers), core), device_id_type=MESH
+        )
+
+    pl.semaphore_signal(barrier, inc=1, device_id=(me, other), device_id_type=MESH)
+
     loads = []
     for i, (src, dst) in enumerate(
-        ((out_proj_hbm, out_proj), (gate_hbm.at[0], gate), (up_hbm.at[0], up), (down_hbm.at[0], down))
+        (
+            (routes_hbm, routes),
+            (weights_hbm, weights),
+            (conv_input_hbm, conv_input),
+            (input_gate_hbm, input_gate),
+            (output_gate_hbm, output_gate),
+            (taps_hbm, taps),
+            (out_proj_hbm, out_proj),
+            (residual_hbm, residual),
+            (gain_hbm, gain),
+            (gate_hbm.at[0], gate),
+            (up_hbm.at[0], up),
+            (down_hbm.at[0], down),
+        )
     ):
         load = pltpu.make_async_copy(src, dst, load_sem.at[i])
         load.start()
         loads.append(load)
 
-    barrier = pltpu.get_barrier_semaphore()
-
-    @pl.loop(1, peers)
-    def _(k):
-        pl.semaphore_signal(
-            barrier, inc=1, device_id=(lax.rem(me + k, peers), core), device_id_type=MESH
-        )
-
-    pl.semaphore_signal(barrier, inc=1, device_id=(me, other), device_id_type=MESH)
+    loads[0].wait()
+    loads[1].wait()
     tops = routes.shape[0]
     ids = lax.broadcasted_iota(jnp.int32, (peers, tokens), 0)
     hots = [(routes[k : k + 1, :] == ids).astype(F32) for k in range(tops)]
@@ -129,6 +160,8 @@
             rest = rest - piece
         spread[g] = jnp.concatenate(pieces, axis=1).astype(BF16)
 
+    for i in range(2, 6):
+        loads[i].wait()
     ext[pl.ds(RIM, length)] = input_gate[...].astype(F32) * conv_input[...].astype(F32)
 
     def gate_rows(lane):
@@ -141,7 +174,7 @@
         return (opened * convolved).astype(BF16)
 
     late = gate_rows(1)
-    loads[0].wait()
+    loads[6].wait()
     proj[1] = dot(late, out_proj[...])
 
     pl.semaphore_wait(barrier, peers)
@@ -191,13 +224,66 @@
     def _():
         proj_copy.start()
 
+    loads[7].wait()
+    loads[8].wait()
     proj_copy.wait_recv()
     stream = residual[...].astype(F32) + (proj[core] + proj_in[...])
     inverse_rms = lax.rsqrt(jnp.mean(stream * stream, axis=-1, keepdims=True) + 1e-06)
     normed = (stream * inverse_rms * gain[...]).astype(BF16)
-    proj_copy.wait_send()
-    proj[core] = stream
-    outgoing[...] = dot(chosen[...], normed).astype(BF16).reshape(peers, rows, width)
+    raw[...] = normed
+
+    mine = me // per_group
+    span_rows = per_group * rows
+    if groups == 4:
+        near = mine // 2 * 2
+        far = lax.rem(near + 2, 4)
+        side = mine - near
+        beside, across, mirror = near + 1 - side, far + side, far + 1 - side
+        middle = lax.rem(mine // 2 + side, 2)
+        order = [
+            mine,
+            beside + middle * (mirror - beside),
+            mirror + middle * (beside - mirror),
+            across,
+        ]
+        back = [mine, beside, mirror, across]
+        sends = [mine, beside]
+        distant = [mirror, across]
+        partner = me + middle * (mirror - mine) * per_group
+    else:
+        order = back = sends = [lax.rem(mine + step, groups) for step in range(groups)]
+        distant = []
+        middle, partner = 0, me
+    column_half = width // 2
+
+    def raw_copy(part_of):
+        cols = pl.ds(part_of * column_half, column_half)
+        return pltpu.make_async_remote_copy(
+            src_ref=raw.at[:, cols],
+            dst_ref=raw_in.at[:, cols],
+            send_sem=raw_send.at[part_of],
+            recv_sem=raw_recv.at[part_of],
+            device_id=(partner, core),
+            device_id_type=MESH,
+        )
+
+    def chosen_copy():
+        return pltpu.make_async_remote_copy(
+            src_ref=chosen.at[pl.ds(pl.multiple_of(far * span_rows, span_rows), 2 * span_rows)],
+            dst_ref=chosen_in,
+            send_sem=chosen_send,
+            recv_sem=chosen_recv,
+            device_id=(partner, core),
+            device_id_type=MESH,
+        )
+
+    if groups == 4:
+
+        @pl.when(middle == 1)
+        def _():
+            chosen_copy().start()
+            for part_of in range(2):
+                raw_copy(part_of).start()
 
     def out_copy(slot, src, target):
         return pltpu.make_async_remote_copy(
@@ -209,34 +295,31 @@
             device_id_type=MESH,
         )
 
-    mine = me // per_group
-    if groups == 4:
-        near = mine // 2 * 2
-        far = lax.rem(near + 2, 4)
-        side = mine - near
-        order = [(far + side, 1), (far + 1 - side, 1)]
-        if active.shape[0] > 2 * half:
-            order = [(near, 2)] + order
-        else:
-            order = [(mine, 1), (near + 1 - side, 1)] + order
-    else:
-        order = [(lax.rem(mine + step, groups), 1) for step in range(groups)]
-    order = [(group * per_group, count * per_group) for group, count in order]
-
-    for first, count in order:
-
-        @pl.loop(0, count)
+    def send_plane(plane):
+        picked = chosen[pl.ds(pl.multiple_of(plane * span_rows, span_rows), span_rows)]
+        slots = dot(picked, normed).astype(BF16).reshape(per_group, rows, width)
+        outgoing[pl.ds(plane * per_group, per_group)] = slots
+
+        @pl.loop(0, per_group)
         def _(i):
-            target = first + lax.rem(me + i, count)
+            target = plane * per_group + lax.rem(me + i, per_group)
 
             @pl.when(target != me)
             def _():
                 out_copy(target, me, target).start()
 
+    for plane in sends:
+        send_plane(plane)
     recv[core, me] = outgoing[me]
-    loads[1].wait()
-    loads[2].wait()
-    loads[3].wait()
+    if groups == 4:
+
+        @pl.when(middle == 0)
+        def _():
+            for plane in distant:
+                send_plane(plane)
+
+    proj_copy.wait_send()
+    proj[core] = stream
 
     def fwd_copy(src, lane):
         return pltpu.make_async_remote_copy(
@@ -260,20 +343,65 @@
 
     in_tile = tile_of(hidden, IN_TILE)
     out_tile = tile_of(width // 2, OUT_TILE)
-
-    for step, (first, count) in enumerate(order):
-        span = pl.ds(first, count)
-        lot = count * rows
+    count = per_group
+    lot = count * rows
+
+    def begin(step):
+        first = order[step] * per_group
 
         @pl.loop(0, count)
         def _(i):
             src = first + lax.rem(me + i, count)
 
-            @pl.when(src != me)
+            @pl.when((src != me) & (src != partner))
             def _():
                 out_copy(src, src, src).wait_recv()
 
             fwd_copy(src, core).start()
+
+    def relay():
+        chosen_copy().wait_recv()
+        for part_of in range(2):
+            raw_copy(part_of).wait_recv()
+            cols = pl.ds(part_of * column_half, column_half)
+            picked = dot(chosen_in[...], raw_in[:, cols]).astype(BF16)
+            outgoing[pl.ds(far * per_group, 2 * per_group), :, cols] = picked.reshape(
+                2 * per_group, rows, column_half
+            )
+
+            @pl.loop(0, 2 * per_group)
+            def _(i):
+                target = near * per_group + lax.rem(me + i, 2 * per_group)
+                slot = lax.rem(target + peers // 2, peers)
+
+                @pl.when(target != me)
+                def _():
+                    pltpu.make_async_remote_copy(
+                        src_ref=outgoing.at[slot, :, cols],
+                        dst_ref=recv.at[core, partner, :, cols],
+                        send_sem=out_send.at[slot],
+                        recv_sem=out_recv.at[partner],
+                        device_id=(target, core),
+                        device_id_type=MESH,
+                    ).start()
+
+        recv[core, partner] = outgoing[lax.rem(me + peers // 2, peers)]
+
+    def part_copy(step, side_of):
+        span = pl.ds(order[step] * per_group, count)
+        part_half = pl.ds(side_of * column_half, column_half)
+        return pltpu.make_async_remote_copy(
+            src_ref=part.at[other, span, :, part_half],
+            dst_ref=part_in.at[span, :, part_half],
+            send_sem=part_send.at[step, side_of],
+            recv_sem=part_recv.at[step, side_of],
+            device_id=(me, other),
+            device_id_type=MESH,
+        )
+
+    def raise_up(step):
+        first = order[step] * per_group
+        span = pl.ds(first, count)
 
         @pl.loop(0, count)
         def _(i):
@@ -285,31 +413,25 @@
             x = recv[:, span].reshape(2 * lot, width)
             g = dot(x, gate[:, cols])
             u = dot(x, up[:, cols])
-            active[pl.ds(0, 2 * lot), cols] = (g * (1.0 / (1.0 + jnp.exp(-g))) * u).astype(BF16)
-
-        copies = []
+            active[:, cols] = (g * (1.0 / (1.0 + jnp.exp(-g))) * u).astype(BF16)
+
+    def bring_down(step):
+        span = pl.ds(order[step] * per_group, count)
         for side_of in range(2):
-            start = side_of * (width // 2)
-
-            @pl.loop(0, width // 2 // out_tile)
+            start = side_of * column_half
+
+            @pl.loop(0, column_half // out_tile)
             def _(n):
                 cols = pl.ds(pl.multiple_of(start + n * out_tile, 128), out_tile)
-                y = dot(active[pl.ds(0, 2 * lot)], down[:, cols]).astype(BF16)
+                y = dot(active[...], down[:, cols]).astype(BF16)
                 part[:, span, :, cols] = y.reshape(2, count, rows, out_tile)
 
-            part_half = pl.ds(start, width // 2)
-            copy = pltpu.make_async_remote_copy(
-                src_ref=part.at[other, span, :, part_half],
-                dst_ref=part_in.at[span, :, part_half],
-                send_sem=part_send.at[step, side_of],
-                recv_sem=part_recv.at[step, side_of],
-                device_id=(me, other),
-                device_id_type=MESH,
-            )
-            copy.start()
-            copies.append(copy)
-        for copy in copies:
-            copy.wait()
+            part_copy(step, side_of).start()
+
+    def tail(step):
+        first = order[step] * per_group
+        for side_of in range(2):
+            part_copy(step, side_of).wait()
 
         @pl.loop(0, count)
         def _(i):
@@ -325,7 +447,29 @@
             def _():
                 ret[me] = halves
 
-    for step, (first, count) in enumerate(order):
+    if groups == 4:
+
+        @pl.when(middle == 1)
+        def _():
+            relay()
+
+    begin(0)
+    for step in range(groups):
+        if step == 0:
+            loads[9].wait()
+            loads[10].wait()
+        raise_up(step)
+        if step > 0:
+            tail(step - 1)
+        else:
+            loads[11].wait()
+        if step < groups - 1:
+            begin(step + 1)
+        bring_down(step)
+    tail(groups - 1)
+
+    for step, plane in enumerate(back):
+        first = plane * per_group
 
         @pl.loop(0, count)
         def _(i):
@@ -337,26 +481,34 @@
 
         for n in range(width // out_tile):
             cols = pl.ds(n * out_tile, out_tile)
-            added = proj[core, :, cols]
-            for g in range(count // per_group):
-                values = ret[pl.ds(first + g * per_group, per_group), :, cols]
-                values = values.reshape(half, out_tile)
-                added = added + dot(
-                    spread[first // per_group + g], jnp.concatenate([values] * 3, axis=0)
-                )
-            if step < len(order) - 1:
+            values = ret[pl.ds(first, count), :, cols].reshape(lot, out_tile)
+            added = proj[core, :, cols] + dot(
+                spread[plane], jnp.concatenate([values] * 3, axis=0)
+            )
+            if step < groups - 1:
                 proj[core, :, cols] = added
             else:
                 out[:, cols] = added.astype(BF16)
 
     @pl.loop(0, peers)
     def _(src):
+        @pl.when((src != me) & (lax.rem(src + middle * (peers // 2), peers) != me))
+        def _():
+            out_copy(src, src, src).wait_send()
+
         @pl.when(src != me)
         def _():
-            out_copy(src, src, src).wait_send()
             ret_copy(src, src, src).wait_send()
 
         fwd_copy(src, core).wait_send()
+
+    if groups == 4:
+
+        @pl.when(middle == 1)
+        def _():
+            chosen_copy().wait_send()
+            for part_of in range(2):
+                raw_copy(part_of).wait_send()
 
     @pl.when(me < peers - 1)
     def _():
@@ -386,16 +538,24 @@
     rows = -(-capacity // 16) * 16
     groups = 4 if peers % 4 == 0 else 1
     half = peers // groups * rows
-    joined = 2 if groups == 4 and half <= 64 else 1
+    relayed = 2 * half if groups == 4 else rows
     dma = pltpu.SemaphoreType.DMA
     vmem = pl.BlockSpec(memory_space=pltpu.VMEM)
     hbm = pl.BlockSpec(memory_space=pltpu.HBM)
     return pl.pallas_call(
         functools.partial(kernel, peers, groups, rows),
         out_shape=jax.ShapeDtypeStruct((tokens, width), BF16),
-        in_specs=[vmem] * 8 + [hbm] * 4,
+        in_specs=[hbm] * 12,
         out_specs=vmem,
         scratch_shapes=[
+            pltpu.VMEM(residual.shape, BF16),
+            pltpu.VMEM(conv_input.shape, BF16),
+            pltpu.VMEM(input_gate.shape, BF16),
+            pltpu.VMEM(output_gate.shape, BF16),
+            pltpu.VMEM(conv_taps.shape, BF16),
+            pltpu.VMEM((1, width), F32),
+            pltpu.VMEM(routes.shape[::-1], jnp.int32),
+            pltpu.VMEM(route_weight.shape[::-1], F32),
             pltpu.VMEM(out_proj.shape, BF16),
             pltpu.VMEM(gate_proj.shape[1:], BF16),
             pltpu.VMEM(up_proj.shape[1:], BF16),
@@ -405,14 +565,21 @@
             pltpu.VMEM((peers * rows, tokens), BF16),
             pltpu.VMEM((2, tokens, width), F32),
             pltpu.VMEM((tokens, width), F32),
+            pltpu.VMEM((tokens, width), BF16),
+            pltpu.VMEM((tokens, width), BF16),
+            pltpu.VMEM((relayed, tokens), BF16),
             pltpu.VMEM((peers, rows, width), BF16),
             pltpu.VMEM((2, peers, rows, width), BF16),
-            pltpu.VMEM((2 * joined * half, hidden), BF16),
+            pltpu.VMEM((2 * half, hidden), BF16),
             pltpu.VMEM((2, peers, rows, width), BF16),
             pltpu.VMEM((peers, rows, width), BF16),
             pltpu.VMEM((peers, rows, width), BF16),
             pltpu.VMEM((groups, tokens, 3 * half), BF16),
-            dma((4,)),
+            dma((12,)),
+            dma((2,)),
+            dma((2,)),
+            dma,
+            dma,
             dma((2,)),
             dma((2,)),
             dma,

time: 62.3 us -> 60 us (0.963)
  the two profiles are of different devices: /device:TPU:12 before, /device:TPU:0 now
where the time goes in v1:
time: 60 us; the launch traced here: 59.8 us
  Pallas kernels  58.1 us (97%)
  local copies, waits for them, and re-layouts  1.67 us (3%)
    pallas_call x1, Pallas kernels, per_device(): pl.pallas_call(functools.partial(kernel, peers, groups, rows), out_shape=...  58.1 us
    unnamed x1, local copies, waits for them, and re-layouts  1.67 us

profile of v1, /device:TPU:0, one launch (start us, length us, event | category | flops | bytes accessed | tf_op | source)
XLA Modules:
  0.0 59.8 jit_solution(1701792064819936758)
XLA Ops:
  0.0 58.1 %mixer_experts.1 = bf16[64,2048]{1,0:T(8,128)(2,1)} custom-call(bf16[64,2048]{1,0:T(8,128)(2,1)} %residual_hbm.1, bf16[128,512]{1,0:T(8,128)(2,1)} %conv_input_hbm.1, bf16[128,512]{1,0:T(8,128)(2,1)} %input_gate_hbm.1, bf16[128,512]{1,0:T(8,128)(2,1)} %output_gate_hbm.1, bf16[3,512]{1,0:T(4,128)(2,1)} %taps_hbm.1, f32[1,2048]{1,0:T(1,128)} %bitcast.3, ...), custom_call_target="tpu_custom_call" | custom-call | tf_op jit(solution)/shard_map/mixer_experts/pallas_call | solution.py:545
  58.1 1.7 %copy.14 = bf16[64,2048]{1,0:T(8,128)(2,1)} copy(bf16[64,2048]{1,0:T(8,128)(2,1)} %mixer_experts.1) | data formatting | bytes 524288

commit v2 on v1

--- a/solution.py
+++ b/solution.py
@@ -44,6 +44,7 @@
     gate_hbm,
     up_hbm,
     down_hbm,
+    out_hbm,
     out,
     residual,
     conv_input,
@@ -72,6 +73,11 @@
     part_in,
     ret,
     spread,
+    spread_in,
+    gather,
+    summed,
+    sum_in,
+    out_copy_sem,
     load_sem,
     rim_send,
     rim_recv,
@@ -89,6 +95,11 @@
     part_recv,
     ret_send,
     ret_recv,
+    spread_send,
+    spread_recv,
+    gather_recv,
+    sum_send,
+    sum_recv,
 ):
     me = lax.axis_index("sp")
     core = lax.axis_index("tp")
@@ -101,6 +112,7 @@
 
     barrier = pltpu.get_barrier_semaphore()
 
+
     @pl.loop(1, peers)
     def _(k):
         pl.semaphore_signal(
@@ -108,6 +120,7 @@
         )
 
     pl.semaphore_signal(barrier, inc=1, device_id=(me, other), device_id_type=MESH)
+    mine = me // per_group
 
     loads = []
     for i, (src, dst) in enumerate(
@@ -232,7 +245,6 @@
     normed = (stream * inverse_rms * gain[...]).astype(BF16)
     raw[...] = normed
 
-    mine = me // per_group
     span_rows = per_group * rows
     if groups == 4:
         near = mine // 2 * 2
@@ -240,18 +252,16 @@
         side = mine - near
         beside, across, mirror = near + 1 - side, far + side, far + 1 - side
         middle = lax.rem(mine // 2 + side, 2)
-        order = [
-            mine,
-            beside + middle * (mirror - beside),
-            mirror + middle * (beside - mirror),
-            across,
-        ]
-        back = [mine, beside, mirror, across]
+        turn = middle * (beside - across)
+        order = [mine, mirror, across + turn, beside - turn]
         sends = [mine, beside]
         distant = [mirror, across]
         partner = me + middle * (mirror - mine) * per_group
+        anchor = me + (across - mine) * per_group
+        shared = across + (1 - middle) * (mirror - across)
+        hub = (mine + (1 - middle) * (beside - mine)) * per_group
     else:
-        order = back = sends = [lax.rem(mine + step, groups) for step in range(groups)]
+        order = sends = [lax.rem(mine + step, groups) for step in range(groups)]
         distant = []
         middle, partner = 0, me
     column_half = width // 2
@@ -277,6 +287,27 @@
             device_id_type=MESH,
         )
 
+    def spread_copy():
+        return pltpu.make_async_remote_copy(
+            src_ref=spread.at[pl.ds(far, 2)],
+            dst_ref=spread_in,
+            send_sem=spread_send,
+            recv_sem=spread_recv,
+            device_id=(anchor, core),
+            device_id_type=MESH,
+        )
+
+    def sum_copy(part_of):
+        cols = pl.ds(part_of * column_half, column_half)
+        return pltpu.make_async_remote_copy(
+            src_ref=summed.at[:, cols],
+            dst_ref=sum_in.at[:, cols],
+            send_sem=sum_send.at[part_of],
+            recv_sem=sum_recv.at[part_of],
+            device_id=(anchor, core),
+            device_id_type=MESH,
+        )
+
     if groups == 4:
 
         @pl.when(middle == 1)
@@ -317,9 +348,32 @@
         def _():
             for plane in distant:
                 send_plane(plane)
+            spread_copy().start()
 
     proj_copy.wait_send()
     proj[core] = stream
+
+    def gather_copy(src, slot, target, part_of):
+        cols = pl.ds(part_of * column_half, column_half)
+        return pltpu.make_async_remote_copy(
+            src_ref=part.at[core, src, :, cols],
+            dst_ref=gather.at[slot, :, cols],
+            send_sem=ret_send.at[src],
+            recv_sem=gather_recv.at[part_of, slot],
+            device_id=(target, core),
+            device_id_type=MESH,
+        )
+
+    def ret_part(src, part_of):
+        cols = pl.ds(part_of * column_half, column_half)
+        return pltpu.make_async_remote_copy(
+            src_ref=part.at[core, src, :, cols],
+            dst_ref=ret.at[me, :, cols],
+            send_sem=ret_send.at[src],
+            recv_sem=ret_recv.at[me],
+            device_id=(src, core),
+            device_id_type=MESH,
+        )
 
     def fwd_copy(src, lane):
         return pltpu.make_async_remote_copy(
@@ -392,7 +446,7 @@
         part_half = pl.ds(side_of * column_half, column_half)
         return pltpu.make_async_remote_copy(
             src_ref=part.at[other, span, :, part_half],
-            dst_ref=part_in.at[span, :, part_half],
+            dst_ref=part_in.at[step % 2, :, :, part_half],
             send_sem=part_send.at[step, side_of],
             recv_sem=part_recv.at[step, side_of],
             device_id=(me, other),
@@ -430,22 +484,63 @@
 
     def tail(step):
         first = order[step] * per_group
-        for side_of in range(2):
-            part_copy(step, side_of).wait()
-
-        @pl.loop(0, count)
-        def _(i):
-            src = first + lax.rem(me + i, count)
-            halves = (part[core, src].astype(F32) + part_in[src].astype(F32)).astype(BF16)
-            part[core, src] = halves
-
-            @pl.when(src != me)
-            def _():
-                ret_copy(src, me, src).start()
-
-            @pl.when(src == me)
-            def _():
-                ret[me] = halves
+        for part_of in range(2):
+            part_copy(step, part_of).wait()
+            cols = pl.ds(part_of * column_half, column_half)
+
+            @pl.loop(0, count)
+            def _(i):
+                place = lax.rem(me + i, count)
+                src = first + place
+                theirs = part_in[step % 2, place, :, cols].astype(F32)
+                mixed = part[core, src, :, cols].astype(F32) + theirs
+                halves = mixed.astype(BF16)
+                part[core, src, :, cols] = halves
+                if groups == 4:
+                    target = hub + lax.rem(src, per_group)
+                    slot = lax.rem(me, 2 * per_group)
+
+                    @pl.when((order[step] != shared) & (src != me))
+                    def _():
+                        ret_part(src, part_of).start()
+
+                    @pl.when((order[step] == shared) & (target != me))
+                    def _():
+                        gather_copy(src, slot, target, part_of).start()
+
+                    @pl.when((order[step] == shared) & (target == me))
+                    def _():
+                        gather[slot, :, cols] = halves
+
+                else:
+
+                    @pl.when(src != me)
+                    def _():
+                        ret_part(src, part_of).start()
+
+                @pl.when(src == me)
+                def _():
+                    ret[me, :, cols] = halves
+
+    def share():
+        spread_copy().wait_recv()
+        for part_of in range(2):
+
+            @pl.loop(0, 2 * per_group)
+            def _(i):
+                @pl.when(near * per_group + i != me)
+                def _():
+                    gather_copy(me, i, me, part_of).wait_recv()
+
+            for n in range(column_half // out_tile):
+                cols = pl.ds(part_of * column_half + n * out_tile, out_tile)
+                added = jnp.zeros((tokens, out_tile), F32)
+                for j in range(2):
+                    values = gather[pl.ds(j * per_group, per_group), :, cols]
+                    values = values.reshape(lot, out_tile)
+                    added = added + dot(spread_in[j], jnp.concatenate([values] * 3, axis=0))
+                summed[:, cols] = added.astype(BF16)
+            sum_copy(part_of).start()
 
     if groups == 4:
 
@@ -459,16 +554,38 @@
             loads[9].wait()
             loads[10].wait()
         raise_up(step)
-        if step > 0:
+        if step == 0:
+            loads[11].wait()
+        if step == 2:
+
+            @pl.when(middle == 1)
+            def _():
+                tail(1)
+
+        elif step > 0:
             tail(step - 1)
-        else:
-            loads[11].wait()
         if step < groups - 1:
             begin(step + 1)
         bring_down(step)
+        if groups == 4 and step == 1:
+
+            @pl.when(middle == 0)
+            def _():
+                tail(1)
+
     tail(groups - 1)
 
-    for step, plane in enumerate(back):
+    if groups == 4:
+
+        @pl.when(middle == 1)
+        def _():
+            share()
+
+    def store(part_of):
+        cols = pl.ds(part_of * column_half, column_half)
+        return pltpu.make_async_copy(out.at[:, cols], out_hbm.at[:, cols], out_copy_sem.at[part_of])
+
+    def add_plane(plane, last):
         first = plane * per_group
 
         @pl.loop(0, count)
@@ -481,14 +598,35 @@
 
         for n in range(width // out_tile):
             cols = pl.ds(n * out_tile, out_tile)
+            part_of = (n + 1) * out_tile // column_half - 1
+            whole = (n + 1) * out_tile % column_half == 0
             values = ret[pl.ds(first, count), :, cols].reshape(lot, out_tile)
             added = proj[core, :, cols] + dot(
                 spread[plane], jnp.concatenate([values] * 3, axis=0)
             )
-            if step < groups - 1:
+            if last:
+                out[:, cols] = added.astype(BF16)
+                if whole:
+                    store(part_of).start()
+            else:
                 proj[core, :, cols] = added
-            else:
-                out[:, cols] = added.astype(BF16)
+
+    for step, plane in enumerate(sends):
+        add_plane(plane, groups != 4 and step == groups - 1)
+    if groups == 4:
+
+        @pl.when(middle == 1)
+        def _():
+            add_plane(mirror, False)
+            add_plane(across, True)
+
+        @pl.when(middle == 0)
+        def _():
+            for part_of in range(2):
+                cols = pl.ds(part_of * column_half, column_half)
+                sum_copy(part_of).wait_recv()
+                out[:, cols] = (proj[core, :, cols] + sum_in[:, cols].astype(F32)).astype(BF16)
+                store(part_of).start()
 
     @pl.loop(0, peers)
     def _(src):
@@ -496,7 +634,9 @@
         def _():
             out_copy(src, src, src).wait_send()
 
-        @pl.when(src != me)
+        held = anchor if groups == 4 else me
+
+        @pl.when((src != me) & ((middle == 0) | (src != held)))
         def _():
             ret_copy(src, src, src).wait_send()
 
@@ -509,11 +649,19 @@
             chosen_copy().wait_send()
             for part_of in range(2):
                 raw_copy(part_of).wait_send()
+                sum_copy(part_of).wait_send()
+
+        @pl.when(middle == 0)
+        def _():
+            spread_copy().wait_send()
 
     @pl.when(me < peers - 1)
     def _():
         for which in range(2):
             rim_copy(which, me + 1).wait_send()
+
+    for part_of in range(2):
+        store(part_of).wait()
 
 
 def per_device(
@@ -539,15 +687,16 @@
     groups = 4 if peers % 4 == 0 else 1
     half = peers // groups * rows
     relayed = 2 * half if groups == 4 else rows
+    grant = 67043328
     dma = pltpu.SemaphoreType.DMA
-    vmem = pl.BlockSpec(memory_space=pltpu.VMEM)
     hbm = pl.BlockSpec(memory_space=pltpu.HBM)
     return pl.pallas_call(
         functools.partial(kernel, peers, groups, rows),
         out_shape=jax.ShapeDtypeStruct((tokens, width), BF16),
         in_specs=[hbm] * 12,
-        out_specs=vmem,
+        out_specs=hbm,
         scratch_shapes=[
+            pltpu.VMEM((tokens, width), BF16),
             pltpu.VMEM(residual.shape, BF16),
             pltpu.VMEM(conv_input.shape, BF16),
             pltpu.VMEM(input_gate.shape, BF16),
@@ -572,9 +721,14 @@
             pltpu.VMEM((2, peers, rows, width), BF16),
             pltpu.VMEM((2 * half, hidden), BF16),
             pltpu.VMEM((2, peers, rows, width), BF16),
-            pltpu.VMEM((peers, rows, width), BF16),
+            pltpu.VMEM((2, peers // groups, rows, width), BF16),
             pltpu.VMEM((peers, rows, width), BF16),
             pltpu.VMEM((groups, tokens, 3 * half), BF16),
+            pltpu.VMEM((2, tokens, 3 * half), BF16),
+            pltpu.VMEM((peers // 2, rows, width), BF16),
+            pltpu.VMEM((tokens, width), BF16),
+            pltpu.VMEM((tokens, width), BF16),
+            dma((2,)),
             dma((12,)),
             dma((2,)),
             dma((2,)),
@@ -592,9 +746,14 @@
             dma((groups, 2)),
             dma((peers,)),
             dma((peers,)),
+            dma,
+            dma,
+            dma((2, peers // 2)),
+            dma((2,)),
+            dma((2,)),
         ],
         compiler_params=pltpu.CompilerParams(
-            collective_id=0, has_side_effects=True, vmem_limit_bytes=67043328
+            collective_id=0, has_side_effects=True, vmem_limit_bytes=grant
         ),
         name="mixer_experts",
     )(

time: 60 us -> 56.7 us (0.945)
  Pallas kernels: 58.1 us -> 54.9 us
    pallas_call x1, Pallas kernels: 58.1 us -> 54.9 us  [per_device(): pl.pallas_call(functools.partial(kernel, peers, groups, rows), out_shape=...]
where the time goes in v2:
time: 56.7 us; the launch traced here: 56.5 us
  Pallas kernels  54.9 us (97%)
  local copies, waits for them, and re-layouts  1.67 us (3%)
    pallas_call x1, Pallas kernels, per_device(): pl.pallas_call(functools.partial(kernel, peers, groups, rows), out_shape=...  54.9 us
    unnamed x1, local copies, waits for them, and re-layouts  1.67 us

profile of v2, /device:TPU:0, one launch (start us, length us, event | category | flops | bytes accessed | tf_op | source)
XLA Modules:
  0.0 56.5 jit_solution(10450467211738689366)
XLA Ops:
  0.0 54.9 %mixer_experts.1 = bf16[64,2048]{1,0:T(8,128)(2,1)} custom-call(bf16[64,2048]{1,0:T(8,128)(2,1)} %residual_hbm.1, bf16[128,512]{1,0:T(8,128)(2,1)} %conv_input_hbm.1, bf16[128,512]{1,0:T(8,128)(2,1)} %input_gate_hbm.1, bf16[128,512]{1,0:T(8,128)(2,1)} %output_gate_hbm.1, bf16[3,512]{1,0:T(4,128)(2,1)} %taps_hbm.1, f32[1,2048]{1,0:T(1,128)} %bitcast.3, ...), custom_call_target="tpu_custom_call" | custom-call | tf_op jit(solution)/shard_map/mixer_experts/pallas_call | solution.py:693
  54.9 1.7 %copy.14 = bf16[64,2048]{1,0:T(8,128)(2,1)} copy(bf16[64,2048]{1,0:T(8,128)(2,1)} %mixer_experts.1) | data formatting | bytes 524288

commit v3 on v2

--- a/solution.py
+++ b/solution.py
@@ -13,7 +13,6 @@
 RIM = 16
 
 
-IN_TILE = 1792
 OUT_TILE = 1024
 
 
@@ -221,22 +220,20 @@
     def _():
         proj_copy.start()
 
-    @pl.when(me == 0)
-    def _():
-        ext[pl.ds(0, RIM)] = jnp.zeros((RIM, channels), F32)
-
-    @pl.when(me > 0)
-    def _():
-        for which in range(2):
-            rim_copy(which, me).wait_recv()
-        ext[pl.ds(0, RIM)] = rim[1].astype(F32) * rim[0].astype(F32)
-
-    proj[0] = dot(gate_rows(0), out_proj[...])
-
-    @pl.when(core == 1)
-    def _():
-        proj_copy.start()
-
+    def early_rows():
+        @pl.when(me == 0)
+        def _():
+            ext[pl.ds(0, RIM)] = jnp.zeros((RIM, channels), F32)
+
+        @pl.when(me > 0)
+        def _():
+            for which in range(2):
+                rim_copy(which, me).wait_recv()
+            ext[pl.ds(0, RIM)] = rim[1].astype(F32) * rim[0].astype(F32)
+
+        proj[0] = dot(gate_rows(0), out_proj[...])
+
+    pl.when(core == 0)(early_rows)
     loads[7].wait()
     loads[8].wait()
     proj_copy.wait_recv()
@@ -328,7 +325,7 @@
 
     def send_plane(plane):
         picked = chosen[pl.ds(pl.multiple_of(plane * span_rows, span_rows), span_rows)]
-        slots = dot(picked, normed).astype(BF16).reshape(per_group, rows, width)
+        slots = dot(picked, raw[...]).astype(BF16).reshape(per_group, rows, width)
         outgoing[pl.ds(plane * per_group, per_group)] = slots
 
         @pl.loop(0, per_group)
@@ -342,16 +339,23 @@
     for plane in sends:
         send_plane(plane)
     recv[core, me] = outgoing[me]
-    if groups == 4:
-
-        @pl.when(middle == 0)
-        def _():
-            for plane in distant:
-                send_plane(plane)
-            spread_copy().start()
+    proj[core] = stream
+
+    def send_far():
+        for plane in distant:
+            send_plane(plane)
+        spread_copy().start()
+
+    if groups == 4:
+        pl.when((middle == 0) & (core == 0))(send_far)
+
+
+    @pl.when(core == 1)
+    def _():
+        early_rows()
+        proj_copy.start()
 
     proj_copy.wait_send()
-    proj[core] = stream
 
     def gather_copy(src, slot, target, part_of):
         cols = pl.ds(part_of * column_half, column_half)
@@ -395,7 +399,7 @@
             device_id_type=MESH,
         )
 
-    in_tile = tile_of(hidden, IN_TILE)
+    cut = -(-hidden // 512) * 256
     out_tile = tile_of(width // 2, OUT_TILE)
     count = per_group
     lot = count * rows
@@ -453,7 +457,7 @@
             device_id_type=MESH,
         )
 
-    def raise_up(step):
+    def raise_up(step, between):
         first = order[step] * per_group
         span = pl.ds(first, count)
 
@@ -461,9 +465,10 @@
         def _(i):
             fwd_copy(first + lax.rem(me + i, count), other).wait_recv()
 
-        @pl.loop(0, hidden // in_tile)
-        def _(n):
-            cols = pl.ds(pl.multiple_of(n * in_tile, in_tile), in_tile)
+        for start, size in ((0, cut), (cut, hidden - cut)):
+            if start:
+                between()
+            cols = pl.ds(start, size)
             x = recv[:, span].reshape(2 * lot, width)
             g = dot(x, gate[:, cols])
             u = dot(x, up[:, cols])
@@ -549,30 +554,17 @@
             relay()
 
     begin(0)
+    if groups == 4:
+        pl.when((middle == 0) & (core == 1))(send_far)
+
     for step in range(groups):
         if step == 0:
             loads[9].wait()
             loads[10].wait()
-        raise_up(step)
-        if step == 0:
-            loads[11].wait()
-        if step == 2:
-
-            @pl.when(middle == 1)
-            def _():
-                tail(1)
-
-        elif step > 0:
-            tail(step - 1)
+        raise_up(step, functools.partial(tail, step - 1) if step > 0 else loads[11].wait)
         if step < groups - 1:
             begin(step + 1)
         bring_down(step)
-        if groups == 4 and step == 1:
-
-            @pl.when(middle == 0)
-            def _():
-                tail(1)
-
     tail(groups - 1)
 
     if groups == 4:
@@ -611,54 +603,61 @@
             else:
                 proj[core, :, cols] = added
 
-    for step, plane in enumerate(sends):
-        add_plane(plane, groups != 4 and step == groups - 1)
+    if groups == 4:
+        add_plane(mine, False)
+
+    @pl.loop(0, peers)
+    def _(src):
+        @pl.when((src != me) & (lax.rem(src + middle * (peers // 2), peers) != me))
+        def _():
+            out_copy(src, src, src).wait_send()
+
+        held = anchor if groups == 4 else me
+
+        @pl.when((src != me) & ((middle == 0) | (src != held)))
+        def _():
+            ret_copy(src, src, src).wait_send()
+
+        fwd_copy(src, core).wait_send()
+
     if groups == 4:
 
         @pl.when(middle == 1)
         def _():
+            chosen_copy().wait_send()
+            for part_of in range(2):
+                raw_copy(part_of).wait_send()
+                sum_copy(part_of).wait_send()
+
+        @pl.when(middle == 0)
+        def _():
+            spread_copy().wait_send()
+
+    @pl.when(me < peers - 1)
+    def _():
+        for which in range(2):
+            rim_copy(which, me + 1).wait_send()
+
+    if groups == 4:
+
+        @pl.when(middle == 1)
+        def _():
             add_plane(mirror, False)
-            add_plane(across, True)
+            add_plane(across, False)
+            add_plane(beside, True)
 
         @pl.when(middle == 0)
         def _():
+            add_plane(beside, False)
             for part_of in range(2):
                 cols = pl.ds(part_of * column_half, column_half)
                 sum_copy(part_of).wait_recv()
                 out[:, cols] = (proj[core, :, cols] + sum_in[:, cols].astype(F32)).astype(BF16)
                 store(part_of).start()
 
-    @pl.loop(0, peers)
-    def _(src):
-        @pl.when((src != me) & (lax.rem(src + middle * (peers // 2), peers) != me))
-        def _():
-            out_copy(src, src, src).wait_send()
-
-        held = anchor if groups == 4 else me
-
-        @pl.when((src != me) & ((middle == 0) | (src != held)))
-        def _():
-            ret_copy(src, src, src).wait_send()
-
-        fwd_copy(src, core).wait_send()
-
-    if groups == 4:
-
-        @pl.when(middle == 1)
-        def _():
-            chosen_copy().wait_send()
-            for part_of in range(2):
-                raw_copy(part_of).wait_send()
-                sum_copy(part_of).wait_send()
-
-        @pl.when(middle == 0)
-        def _():
-            spread_copy().wait_send()
-
-    @pl.when(me < peers - 1)
-    def _():
-        for which in range(2):
-            rim_copy(which, me + 1).wait_send()
+    else:
+        for step, plane in enumerate(sends):
+            add_plane(plane, step == groups - 1)
 
     for part_of in range(2):
         store(part_of).wait()

time: 56.7 us -> 56.3 us (level)
  no operation moved by 1% of the time
where the time goes in v3:
time: 56.3 us; the launch traced here: 56.1 us
  Pallas kernels  54.5 us (97%)
  local copies, waits for them, and re-layouts  1.67 us (3%)
    pallas_call x1, Pallas kernels, per_device(): pl.pallas_call(functools.partial(kernel, peers, groups, rows), out_shape=...  54.5 us
    unnamed x1, local copies, waits for them, and re-layouts  1.67 us

profile of v3, /device:TPU:0, one launch (start us, length us, event | category | flops | bytes accessed | tf_op | source)
XLA Modules:
  0.0 56.1 jit_solution(1876205570491163071)
XLA Ops:
  0.0 54.5 %mixer_experts.1 = bf16[64,2048]{1,0:T(8,128)(2,1)} custom-call(bf16[64,2048]{1,0:T(8,128)(2,1)} %residual_hbm.1, bf16[128,512]{1,0:T(8,128)(2,1)} %conv_input_hbm.1, bf16[128,512]{1,0:T(8,128)(2,1)} %input_gate_hbm.1, bf16[128,512]{1,0:T(8,128)(2,1)} %output_gate_hbm.1, bf16[3,512]{1,0:T(4,128)(2,1)} %taps_hbm.1, f32[1,2048]{1,0:T(1,128)} %bitcast.3, ...), custom_call_target="tpu_custom_call" | custom-call | tf_op jit(solution)/shard_map/mixer_experts/pallas_call | solution.py:692
  54.5 1.7 %copy.14 = bf16[64,2048]{1,0:T(8,128)(2,1)} copy(bf16[64,2048]{1,0:T(8,128)(2,1)} %mixer_experts.1) | data formatting | bytes 524288
